TPU v7x, 32 devices: a whole 2x2x4 slice. The times are simulated.
32 devices in a mesh: sp: 8 (over z, x), tp: 4 (over y, core).
Axes of the slice: x: 2, y: 2, z: 4, core: 2. Of those that a mesh axis runs over, the one named last changes fastest.
Arguments:
- tokens: bfloat16 [8, 80, 4096], P(None, 'sp', 'tp'), may hold values from -6 to 6
- latent_down_weight: bfloat16 [4096, 512], replicated, may hold values from -0.09375 to 0.09375
- w_rope_key: bfloat16 [4096, 64], replicated, may hold values from -0.09375 to 0.09375
- latent_norm_gain: float32 [512], replicated, may hold values from 0.1 to 1.9
- key_up_weight: bfloat16 [512, 4096], P(None, 'tp'), may hold values from -0.25 to 0.25
- value_up_weight: bfloat16 [512, 4096], P(None, 'tp'), may hold values from -0.25 to 0.25
- cached_latent_rows: bfloat16 [8, 32768, 512], P('sp', 'tp'), may hold values from -6 to 6
- past_rope: bfloat16 [8, 32768, 64], P('sp', 'tp'), may hold values from -6 to 6
- query_nope: bfloat16 [8, 4096], P('sp', 'tp'), may hold values from -8 to 8
- query_rope: bfloat16 [8, 2048], P('sp', 'tp'), may hold values from -300 to 300
Outputs:
- new_keys: bfloat16 [8, 80, 4096], P('sp', None, 'tp')
- new_values: bfloat16 [8, 80, 4096], P('sp', None, 'tp')
- new_rope: bfloat16 [8, 80, 64], P('sp')
- attended: bfloat16 [8, 4096], P('sp', 'tp')
All inputs are finite; a program needn't handle non-finite values.
Results may differ from a plain program's by a relative error of at most 0.0085.
Values may be sent and summed in bfloat16 or wider, within the bound.
A program may use at most 64 MiB of HBM per device.

v0:
```python
import jax
import jax.numpy as jnp
from jax import lax
from jax.sharding import PartitionSpec as P

PLAIN_KEY_WIDTH = 128
ROPE = 64
VALUE_WIDTH = 128
PAST_POSITIONS = 32768
epsilon = 1e-06
rope_theta = 10000.0


def combined_all(part, axis, combine):
    gathered = jax.tree.map(lambda a: lax.all_gather(a, axis), part)

    def take(source):
        return jax.tree.map(lambda a: lax.dynamic_index_in_dim(a, source, 0, False), gathered)

    return lax.fori_loop(
        1, lax.axis_size(axis), lambda source, state: combine(state, take(source)), take(0)
    )


def rotate(values, positions):
    halfway = values.shape[-1] // 2
    frequency = rope_theta ** (-jnp.arange(halfway, dtype=jnp.float32) / halfway)
    angles = positions[:, None] * frequency
    first = values[..., :halfway]
    second = values[..., halfway:]
    return jnp.concatenate(
        [
            first * jnp.cos(angles) - second * jnp.sin(angles),
            first * jnp.sin(angles) + second * jnp.cos(angles),
        ],
        axis=-1,
    )


def combine_parts(first, second):
    highest = jnp.maximum(first[0], second[0])
    scale_first = jnp.exp(first[0] - highest)
    scale_second = jnp.exp(second[0] - highest)
    total = first[1] * scale_first + second[1] * scale_second
    summed = first[2] * scale_first[..., None] + second[2] * scale_second[..., None]
    return (highest, total, summed)


def on_device(
    tokens,
    latent_down_weight,
    w_rope_key,
    latent_norm_gain,
    key_up_weight,
    value_up_weight,
    cached_latent_rows,
    past_rope,
    query_nope,
    query_rope,
):
    rows_here = lax.all_to_all(tokens, "sp", split_axis=0, concat_axis=1, tiled=True)
    prompts, per_seq, features = rows_here.shape
    row_count = prompts * per_seq
    latent_width = latent_down_weight.shape[1]
    turn_width = w_rope_key.shape[1]
    factor = (PLAIN_KEY_WIDTH + ROPE) ** (-0.5)
    fragment = lax.all_gather(rows_here, "tp", axis=2, tiled=True)
    columns = fragment.shape[2]
    flat_rows = fragment.reshape(row_count, columns)
    latent_raw = jnp.dot(flat_rows, latent_down_weight, preferred_element_type=jnp.float32)
    rope_raw = jnp.dot(flat_rows, w_rope_key, preferred_element_type=jnp.float32)
    scale = lax.rsqrt(jnp.mean(latent_raw * latent_raw, axis=-1, keepdims=True) + epsilon)
    latent = (latent_raw * scale * latent_norm_gain).astype(jnp.bfloat16)
    positions = (PAST_POSITIONS + jnp.arange(per_seq)).astype(jnp.float32)
    rope_local = rotate(rope_raw.reshape(prompts, per_seq, turn_width), positions).astype(
        jnp.bfloat16
    )
    keys_local = (
        jnp.dot(latent, key_up_weight, preferred_element_type=jnp.float32)
        .astype(jnp.bfloat16)
        .reshape(prompts, per_seq, key_up_weight.shape[1])
    )
    values_local = (
        jnp.dot(latent, value_up_weight, preferred_element_type=jnp.float32)
        .astype(jnp.bfloat16)
        .reshape(prompts, per_seq, value_up_weight.shape[1])
    )
    new_keys, new_values, new_rope = (keys_local, values_local, rope_local)
    owned = query_nope.shape[0]
    heads_local = query_nope.shape[1] // PLAIN_KEY_WIDTH
    query_own = query_nope.reshape(owned, heads_local, PLAIN_KEY_WIDTH)
    turn_own = query_rope.reshape(owned, heads_local, ROPE)
    head_keys = key_up_weight.reshape(latent_width, heads_local, PLAIN_KEY_WIDTH)
    query_latent = jnp.einsum(
        "shd,khd->shk", query_own, head_keys, preferred_element_type=jnp.float32
    ).astype(jnp.bfloat16)
    every_latent, every_turn = (
        lax.all_gather(query_latent, "tp", axis=1, tiled=True),
        lax.all_gather(turn_own, "tp", axis=1, tiled=True),
    )
    past_scores = jnp.einsum(
        "shk,spk->shp", every_latent, cached_latent_rows, preferred_element_type=jnp.float32
    )
    past_scores = (
        past_scores
        + jnp.einsum("shd,spd->shp", every_turn, past_rope, preferred_element_type=jnp.float32)
    ) * factor
    local_peak = jnp.max(past_scores, axis=-1)
    local_weight = jnp.exp(past_scores - local_peak[:, :, None])
    local_total = jnp.sum(local_weight, axis=-1)
    local_latent = jnp.einsum(
        "shp,spk->shk",
        local_weight.astype(jnp.bfloat16),
        cached_latent_rows,
        preferred_element_type=jnp.float32,
    )
    peak_all, total_all, latent_all = combined_all(
        (local_peak, local_total, local_latent), "tp", combine_parts
    )
    start = lax.axis_index("tp") * heads_local
    past_peak = lax.dynamic_slice_in_dim(peak_all, start, heads_local, 1)
    past_total = lax.dynamic_slice_in_dim(total_all, start, heads_local, 1)
    past_sum = lax.dynamic_slice_in_dim(latent_all, start, heads_local, 1)
    fresh = new_keys.shape[1]
    new_scores = jnp.einsum(
        "shd,sphd->shp",
        query_own,
        new_keys.reshape(owned, fresh, heads_local, PLAIN_KEY_WIDTH),
        preferred_element_type=jnp.float32,
    )
    new_scores = (
        new_scores
        + jnp.einsum("shd,spd->shp", turn_own, new_rope, preferred_element_type=jnp.float32)
    ) * factor
    peak = jnp.maximum(past_peak, jnp.max(new_scores, axis=-1))
    past_share = jnp.exp(past_peak - peak)
    new_weight = jnp.exp(new_scores - peak[:, :, None])
    denominator = past_total * past_share + jnp.sum(new_weight, axis=-1)
    latent_sum = (past_sum * past_share[..., None]).astype(jnp.bfloat16)
    head_values = value_up_weight.reshape(latent_width, heads_local, VALUE_WIDTH)
    past_out = jnp.einsum(
        "shk,khd->shd", latent_sum, head_values, preferred_element_type=jnp.float32
    )
    new_out = jnp.einsum(
        "shp,sphd->shd",
        new_weight.astype(jnp.bfloat16),
        new_values.reshape(owned, fresh, heads_local, VALUE_WIDTH),
        preferred_element_type=jnp.float32,
    )
    attended = (
        ((past_out + new_out) / denominator[:, :, None])
        .astype(jnp.bfloat16)
        .reshape(owned, heads_local * VALUE_WIDTH)
    )
    return (new_keys, new_values, new_rope, attended)


def solution(mesh):
    in_specs = (
        P(None, "sp", "tp"),
        P(),
        P(),
        P(),
        P(None, "tp"),
        P(None, "tp"),
        P("sp", "tp", None),
        P("sp", "tp", None),
        P("sp", "tp"),
        P("sp", "tp"),
    )
    out_specs = (P("sp", None, "tp"), P("sp", None, "tp"), P("sp", None, None), P("sp", "tp"))
    return jax.shard_map(
        on_device, mesh=mesh, in_specs=in_specs, out_specs=out_specs, check_vma=False
    )
```

profile of v0, /device:TPU:0, one launch (start us, length us, event | category | flops | bytes accessed | tf_op | source)
XLA Modules:
  0.0 66.8 jit_solution(9695988542635753334)
XLA Ops:
  0.6 1.8 %copy.21 = bf16[8,10,1024]{2,1,0:T(8,128)(2,1)} copy(bf16[8,10,1024]{2,0,1:T(8,128)(2,1)} %param.12) | data formatting | bytes 327680 | tf_op args[0]
  2.4 7.3 %all-to-all-start = ((bf16[8,10,1024]{2,1,0:T(8,128)(2,1)}), bf16[8,10,1024]{2,1,0:T(8,128)(2,1)}, u32[]{:S(2)}, u32[]{:S(2)}) async-start(bf16[8,10,1024]{2,1,0:T(8,128)(2,1)} %copy.21), calls=%async_computation | async-start | bytes 524288 | tf_op jit(solution)/shard_map/all_to_all | solution.py:61
  9.7 0.7 %reduce.8 = bf16[512]{0:T(512)(128)(2,1)S(1)} reduce(bf16[1,512]{1,0:T(2,128)(2,1)} %param.21, bf16[]{:T(256)} %constant.97), dimensions={0}, to_apply=%param.21.reduce_sub_computation | reduce | bytes 2050 | tf_op args[9]
  10.5 5.2 %all_gather.29 = bf16[1,32,64]{2,1,0:T(8,128)(2,1)S(1)} all-gather(bf16[1,8,64]{2,1,0:T(8,128)(2,1)S(1)} %reshape.326), channel_id=1, replica_groups=mesh['sp'=8,'tp'=4] {'tp'}, dimensions={1}, use_global_device_ids=true | all-gather | bytes 5120 | tf_op jit(solution)/shard_map/all_gather | solution.py:99
  15.7 1.6 %fusion.18 = bf16[8,1,512]{2,1,0:T(2,128)(2,1)S(1)} fusion(bf16[1,1024]{1,0:T(2,128)(2,1)} %param.20, bf16[512,1024]{1,0:T(8,128)(2,1)} %param.16), kind=kOutput, calls=%fused_computation.28 | convolution fusion | flops 1048576 | bytes 1058816 | tf_op jit(solution)/shard_map/shd,khd->shk/dot_general | solution.py:94
  17.3 5.2 %all-gather = bf16[32,512]{1,0:T(8,128)(2,1)S(1)} all-gather(bf16[8,512]{1,0:T(8,128)(2,1)S(1)} %bitcast.161), channel_id=2, replica_groups=mesh['sp'=8,'tp'=4] {'tp'}, dimensions={0}, use_global_device_ids=true | all-gather | bytes 40960 | tf_op jit(solution)/shard_map/all_gather | solution.py:98
  22.5 5.9 %fusion.11 = f32[32,8192]{1,0:T(8,128)S(1)} fusion(bf16[32,512]{1,0:T(8,128)(2,1)S(1)} %all-gather, bf16[1,8192,512]{2,1,0:T(8,128)(2,1)} %param.18), kind=kOutput, calls=%fused_computation.17 | convolution fusion | flops 268435456 | bytes 9469952 | tf_op jit(solution)/shard_map/shk,spk->shp/dot_general | solution.py:101
  28.4 0.4 fusion.64
  28.8 0.4 fusion.23
  29.2 0.6 dynamic-slice
  30.5 0.2 dynamic-update-slice
  30.9 7.1 %all-reduce.2 = (f32[128]{0:T(128)S(1)}, f32[128]{0:T(128)S(1)}) all-reduce(f32[128]{0:T(128)S(1)} %dynamic-update-slice, f32[128]{0:T(128)S(1)} %dynamic-update-slice.1), channel_id=3, replica_groups=mesh['sp'=8,'tp'=4] {'tp'}, use_global_device_ids=true, to_apply=%add | all-reduce | flops 256 | bytes 2048
  38.2 5.1 %fusion.9 = f32[32,512]{1,0:T(8,128)S(1)} fusion(bf16[1,8192,512]{2,1,0:T(8,128)(2,1)} %param.18, f32[32,8192]{1,0:T(8,128)S(1)} %get-tuple-element.237, f32[32]{0:T(128)S(1)} %get-tuple-element.236), kind=kOutput, calls=%fused_computation.15 | convolution fusion | flops 268959744 | bytes 9502848 | tf_op jit(solution)/shard_map/shp,spk->shk/dot_general | solution.py:111
  43.2 5.9 %all-gather.3 = f32[128,512]{1,0:T(8,128)S(1)} all-gather(f32[32,512]{1,0:T(8,128)S(1)} %fusion.9), channel_id=5, replica_groups=mesh['sp'=8,'tp'=4] {'tp'}, dimensions={0}, use_global_device_ids=true | all-gather | bytes 327680 | tf_op jit(solution)/shard_map/all_gather | solution.py:15
  49.2 0.5 while.19
  49.7 1.0 %all_to_all.10 = bf16[1,80,1024]{2,1,0:T(8,128)(2,1)S(1)} reshape(bf16[8,10,1024]{2,1,0:T(8,128)(2,1)} %all-to-all-done) | data formatting | bytes 327680 | tf_op jit(solution)/shard_map/all_to_all | solution.py:61
  50.7 8.0 %all_gather.27 = bf16[1,80,4096]{2,1,0:T(8,128)(2,1)S(1)} all-gather(bf16[1,80,1024]{2,1,0:T(8,128)(2,1)S(1)} %all_to_all.10), channel_id=1, replica_groups=mesh['sp'=8,'tp'=4] {'tp'}, dimensions={2}, use_global_device_ids=true | all-gather | bytes 819200 | tf_op jit(solution)/shard_map/all_gather | solution.py:67
  58.7 3.1 %multiply_reduce_fusion = (f32[80]{0:T(128)S(1)}, f32[80,512]{1,0:T(8,128)S(1)}) fusion(bf16[4096,512]{1,0:T(8,128)(2,1)} %param.13, bf16[1,80,4096]{2,1,0:T(8,128)(2,1)S(1)} %all_gather.27), kind=kOutput, calls=%fused_computation.46 | convolution fusion | flops 335626176 | bytes 5013824 | tf_op jit(solution)/shard_map/dot_general | solution.py:70
  61.9 0.4 convolution_convert_fusion.1
  62.5 1.4 %convolution_bitcast_fusion = f32[1,80,64]{1,2,0:T(8,128)S(1)} fusion(bf16[4096,64]{0,1:T(8,128)(2,1)} %param.14, bf16[1,80,4096]{2,1,0:T(8,128)(2,1)S(1)} %all_gather.27), kind=kOutput, calls=%fused_computation.21 | convolution fusion | flops 41943040 | bytes 1200128 | tf_op jit(solution)/shard_map/dot_general | solution.py:71
  63.9 0.4 convolution_convert_fusion
  64.4 0.6 pad_maximum_fusion
  65.7 0.3 fusion.15
  66.2 0.6 copy.64
  (51 shorter events, 2.2 us)
Async XLA Ops:
  0.6 27.8 %copy-start = (bf16[1,8192,64]{1,2,0:T(8,128)(2,1)S(1)}, bf16[1,8192,64]{1,2,0:T(8,128)(2,1)}, u32[]{:S(2)}) copy-start(bf16[1,8192,64]{1,2,0:T(8,128)(2,1)} %param.19) | copy-start | bytes 3145732
  2.4 47.3 %all-to-all-start = ((bf16[8,10,1024]{2,1,0:T(8,128)(2,1)}), bf16[8,10,1024]{2,1,0:T(8,128)(2,1)}, u32[]{:S(2)}, u32[]{:S(2)}) async-start(bf16[8,10,1024]{2,1,0:T(8,128)(2,1)} %copy.21), calls=%async_computation | async-start | bytes 524288 | tf_op jit(solution)/shard_map/all_to_all | solution.py:61
  22.5 6.7 %copy-start.7 = (u32[32]{0:T(128)S(1)}, u32[32]{0:T(128)}, u32[]{:S(2)}) copy-start(u32[32]{0:T(128)} %constant.87) | copy-start | bytes 388
  38.2 23.7 %copy-start.1 = (bf16[512,1024]{1,0:T(8,128)(2,1)S(1)}, bf16[512,1024]{1,0:T(8,128)(2,1)}, u32[]{:S(2)}) copy-start(bf16[512,1024]{1,0:T(8,128)(2,1)} %param.16) | copy-start | bytes 3145732
  38.2 23.7 %copy-start.5 = (f32[512]{0:T(512)S(1)}, f32[512]{0:T(512)}, u32[]{:S(2)}) copy-start(f32[512]{0:T(512)} %param.15) | copy-start | bytes 6148
  43.2 19.0 %copy-start.6 = (bf16[1,1024]{1,0:T(2,128)(2,1)S(1)}, bf16[1,1024]{1,0:T(2,128)(2,1)}, u32[]{:S(2)}) copy-start(bf16[1,1024]{1,0:T(2,128)(2,1)} %param.20) | copy-start | bytes 6148
  43.2 20.7 %copy-start.2 = (bf16[512,1024]{1,0:T(8,128)(2,1)S(1)}, bf16[512,1024]{1,0:T(8,128)(2,1)}, u32[]{:S(2)}) copy-start(bf16[512,1024]{1,0:T(8,128)(2,1)} %param.17) | copy-start | bytes 3145732
  62.3 4.5 %copy-start.3 = (bf16[80,1024]{1,0:T(8,128)(2,1)}, bf16[80,1024]{1,0:T(8,128)(2,1)S(1)}, u32[]{:S(2)}) copy-start(bf16[80,1024]{1,0:T(8,128)(2,1)S(1)} %convolution_convert_fusion.1) | copy-start | bytes 491524
  64.3 2.6 %copy-start.4 = (bf16[80,1024]{1,0:T(8,128)(2,1)}, bf16[80,1024]{1,0:T(8,128)(2,1)S(1)}, u32[]{:S(2)}) copy-start(bf16[80,1024]{1,0:T(8,128)(2,1)S(1)} %convolution_convert_fusion) | copy-start | bytes 491524
where the time goes:
time: 67.3 us; the launch traced here: 66.8 us
  blocking collectives  31.4 us (47%)
  matrix products  19.1 us (28%)
  starting transfers between devices  7.28 us (11%)
  local copies, waits for them, and re-layouts  4.87 us (7%)
  other arithmetic  2.69 us (4%)
  between operations  1.45 us (2%)
    all_gather x1, blocking collectives, on_device(): fragment = lax.all_gather(rows_here, 'tp', axis=2, tiled=True)  7.99 us
    all_to_all x1, starting transfers between devices, on_device(): lax.all_to_all(tokens, 'sp', split_axis=0, concat_axis=1, tiled=True)  7.28 us
    unnamed x1, blocking collectives  7.09 us
    dot_general x1, matrix products, on_device(): jnp.einsum('shk,spk->shp', every_latent, cached_latent_rows, preferred_el...  5.92 us
    all_gather x1, blocking collectives, combined_all(): gathered = jax.tree.map(lambda a: lax.all_gather(a, axis), part)  5.91 us
    all_gather x1, blocking collectives, on_device(): lax.all_gather(query_latent, 'tp', axis=1, tiled=True)  5.19 us
    all_gather x1, blocking collectives, on_device(): lax.all_gather(turn_own, 'tp', axis=1, tiled=True)  5.18 us
    dot_general x1, matrix products, on_device(): jnp.einsum('shp,spk->shk', local_weight.astype(jnp.bfloat16), cached_late...  5.06 us
  transfers between devices with their start and end apart: 1, of which 0 were waited for; matrix products, arithmetic and copies ran while one was open for 24% of the time, Pallas kernels for 0%

commit v1 on v0

--- a/solution.py
+++ b/solution.py
@@ -9,6 +9,33 @@
 PAST_POSITIONS = 32768
 epsilon = 1e-06
 rope_theta = 10000.0
+
+
+def part_frames(z_in, axis_no, tile_in):
+    k_now, kept_arr = (z_in.shape[:axis_no], z_in.shape[axis_no + 1 :])
+    side_arr = z_in.reshape(*k_now, tile_in, -1, *kept_arr)
+    return jnp.moveaxis(side_arr, axis_no, 0)
+
+
+def values_detail(target, out_dim):
+    target = jnp.moveaxis(target, 0, out_dim)
+    e_next = target.shape
+    return target.reshape(
+        *e_next[:out_dim], e_next[out_dim] * e_next[out_dim + 1], *e_next[out_dim + 2 :]
+    )
+
+
+def _perform_wires(obj, axis_name, u, vector):
+    low, now = (lax.axis_size(axis_name), lax.axis_index(axis_name))
+    parts_out = part_frames(obj, u, low)
+    inbox = [parts_out[now]]
+    for jj in range(1, low):
+        near = parts_out[(now + jj) % low]
+        prior = lax.ppermute(near, axis_name, [(d, (d + jj) % low) for d in range(low)])
+        inbox.append(prior)
+    o_now = jnp.stack(inbox)
+    parts_out = o_now[(now - jnp.arange(low)) % low]
+    return values_detail(parts_out, vector)
 
 
 def combined_all(part, axis, combine):
@@ -58,7 +85,7 @@
     query_nope,
     query_rope,
 ):
-    rows_here = lax.all_to_all(tokens, "sp", split_axis=0, concat_axis=1, tiled=True)
+    rows_here = _perform_wires(tokens, "sp", 0, 1)
     prompts, per_seq, features = rows_here.shape
     row_count = prompts * per_seq
     latent_width = latent_down_weight.shape[1]

time: 67.3 us -> 96.7 us (1.44)
  local copies, waits for them, and re-layouts: 4.87 us -> 23.6 us
  other arithmetic: 2.69 us -> 10.1 us
  starting transfers between devices: 7.28 us -> 13.8 us
  matrix products: 19.1 us -> 15.9 us
    ppermute x0 -> x7, starting transfers between devices: none -> 13.8 us  [_perform_wires(): lax.ppermute(near, axis_name, [(d, (d + jj) % low) for d in range(low)])]
    unnamed x23 -> x52, local copies, waits for them, and re-layouts: 3.5 us -> 13.5 us
    all_to_all x1 -> x0, starting transfers between devices: 7.28 us -> none  [on_device(): lax.all_to_all(tokens, 'sp', split_axis=0, concat_axis=1, tiled=True)]
    exp x3, other arithmetic: 0.07 us -> 3.78 us  [combine_parts(): scale_second = jnp.exp(second[0] - highest)]
    dot_general x1, matrix products: 5.06 us -> 1.62 us  [on_device(): jnp.einsum('shp,spk->shk', local_weight.astype(jnp.bfloat16), cached_late...]
    another operation x1 -> x3, local copies, waits for them, and re-layouts: 0.08 us -> 2.66 us
    squeeze x0 -> x1, local copies, waits for them, and re-layouts: none -> 2.24 us  [_perform_wires(): near = parts_out[(now + jj) % low]]
    mul x3, other arithmetic: 0.03 us -> 2 us  [combine_parts(): first[2] * scale_first[..., None] + second[2] * scale_second[..., None]]
  transfers between devices with their start and end apart: 1 -> 7, of which waited for: 0 -> 0; matrix products, arithmetic and copies ran while one was open for 24% -> 37% of each run, Pallas kernels for 0% -> 0%
where the time goes in v1:
time: 96.7 us; the launch traced here: 96 us
  blocking collectives  30.8 us (32%)
  local copies, waits for them, and re-layouts  23.6 us (24%)
  matrix products  15.9 us (16%)
  starting transfers between devices  13.8 us (14%)
  other arithmetic  10.1 us (10%)
  between operations  1.72 us (2%)
    ppermute x7, starting transfers between devices, _perform_wires(): lax.ppermute(near, axis_name, [(d, (d + jj) % low) for d in range(low)])  13.8 us
    unnamed x52, local copies, waits for them, and re-layouts  13.5 us
    all_gather x1, blocking collectives, on_device(): fragment = lax.all_gather(rows_here, 'tp', axis=2, tiled=True)  7.63 us
    unnamed x1, blocking collectives  7.09 us
    dot_general x1, matrix products, on_device(): jnp.einsum('shk,spk->shp', every_latent, cached_latent_rows, preferred_el...  6.05 us
    all_gather x1, blocking collectives, combined_all(): gathered = jax.tree.map(lambda a: lax.all_gather(a, axis), part)  5.76 us
    all_gather x1, blocking collectives, on_device(): lax.all_gather(query_latent, 'tp', axis=1, tiled=True)  5.19 us
    all_gather x1, blocking collectives, on_device(): lax.all_gather(turn_own, 'tp', axis=1, tiled=True)  5.18 us
  transfers between devices with their start and end apart: 7, of which 0 were waited for; matrix products, arithmetic and copies ran while one was open for 37% of the time, Pallas kernels for 0%

profile of v1, /device:TPU:0, one launch (start us, length us, event | category | flops | bytes accessed | tf_op | source)
XLA Modules:
  0.0 96.0 jit_solution(8943003938503257793)
XLA Ops:
  0.7 2.2 %constant_dynamic-slice_fusion.4 = (bf16[1,10,1024]{2,0,1:T(2,128)(2,1)S(1)}, bf16[1,10,1024]{2,0,1:T(2,128)(2,1)S(1)}, bf16[1,10,1024]{2,0,1:T(2,128)(2,1)S(1)}...) fusion(bf16[8,10,1024]{2,0,1:T(8,128)(2,1)} %param.12, ...), kind=kLoop, calls=%fused_computation.89 | loop fusion | bytes 327712 | tf_op jit(solution)/shard_map/squeeze | solution.py:33
  3.6 3.0 %collective-permute-start = (bf16[1,10,1024]{2,1,0:T(8,128)(2,1)}, bf16[1,10,1024]{2,1,0:T(8,128)(2,1)}, u32[]{:S(2)}, u32[]{:S(2)}) collective-permute-start(bf16[1,10,1024]{2,1,0:T(8,128)(2,1)} %copy.46), channel_id=1, source_target_pairs={{0,4},{4,8},{8,12},{12,16},{16,20},{20,24},{24,28},{28,0},{1,5},{5... | collective-permute-start | bytes 61448 | tf_op jit(solution)/shard_map/ppermute | solution.py:34
  7.2 1.6 %collective-permute-start.1 = (bf16[1,10,1024]{2,1,0:T(8,128)(2,1)}, bf16[1,10,1024]{2,1,0:T(8,128)(2,1)}, u32[]{:S(2)}, u32[]{:S(2)}) collective-permute-start(bf16[1,10,1024]{2,1,0:T(8,128)(2,1)} %copy.47), channel_id=1, source_target_pairs={{0,8},{4,12},{8,16},{12,20},{16,24},{20,28},{24,0},{28,4},{1,9},{5... | collective-permute-start | bytes 61448 | tf_op jit(solution)/shard_map/ppermute | solution.py:34
  9.4 2.6 %collective-permute-start.2 = (bf16[1,10,1024]{2,1,0:T(8,128)(2,1)}, bf16[1,10,1024]{2,1,0:T(8,128)(2,1)}, u32[]{:S(2)}, u32[]{:S(2)}) collective-permute-start(bf16[1,10,1024]{2,1,0:T(8,128)(2,1)} %copy.48), channel_id=1, source_target_pairs={{0,12},{4,16},{8,20},{12,24},{16,28},{20,0},{24,4},{28,8},{1,13},{... | collective-permute-start | bytes 61448 | tf_op jit(solution)/shard_map/ppermute | solution.py:34
  14.4 2.6 %collective-permute-start.4 = (bf16[1,10,1024]{2,1,0:T(8,128)(2,1)}, bf16[1,10,1024]{2,1,0:T(8,128)(2,1)}, u32[]{:S(2)}, u32[]{:S(2)}) collective-permute-start(bf16[1,10,1024]{2,1,0:T(8,128)(2,1)} %copy.50), channel_id=1, source_target_pairs={{0,20},{4,24},{8,28},{12,0},{16,4},{20,8},{24,12},{28,16},{1,21},{... | collective-permute-start | bytes 61448 | tf_op jit(solution)/shard_map/ppermute | solution.py:34
  19.0 5.2 %all_gather.29 = bf16[1,32,64]{2,1,0:T(8,128)(2,1)S(1)} all-gather(bf16[1,8,64]{2,1,0:T(8,128)(2,1)S(1)} %reshape.388), channel_id=1, replica_groups=mesh['sp'=8,'tp'=4] {'tp'}, dimensions={1}, use_global_device_ids=true | all-gather | bytes 5120 | tf_op jit(solution)/shard_map/all_gather | solution.py:126
  24.2 1.8 %fusion.18 = bf16[8,1,512]{2,1,0:T(2,128)(2,1)S(1)} fusion(bf16[1,1024]{1,0:T(2,128)(2,1)} %param.20, bf16[512,1024]{1,0:T(8,128)(2,1)} %param.16), kind=kOutput, calls=%fused_computation.29 | convolution fusion | flops 1048576 | bytes 1058816 | tf_op jit(solution)/shard_map/shd,khd->shk/dot_general | solution.py:121
  25.9 5.2 %all-gather = bf16[32,512]{1,0:T(8,128)(2,1)S(1)} all-gather(bf16[8,512]{1,0:T(8,128)(2,1)S(1)} %bitcast.185), channel_id=2, replica_groups=mesh['sp'=8,'tp'=4] {'tp'}, dimensions={0}, use_global_device_ids=true | all-gather | bytes 40960 | tf_op jit(solution)/shard_map/all_gather | solution.py:125
  31.1 6.1 %fusion.11 = f32[32,8192]{1,0:T(8,128)S(1)} fusion(bf16[32,512]{1,0:T(8,128)(2,1)S(1)} %all-gather, bf16[1,8192,512]{2,1,0:T(8,128)(2,1)} %param.18), kind=kOutput, calls=%fused_computation.18 | convolution fusion | flops 268435456 | bytes 9469952 | tf_op jit(solution)/shard_map/shk,spk->shp/dot_general | solution.py:128
  38.0 1.6 %fusion.9 = f32[32,512]{1,0:T(8,128)S(1)} fusion(bf16[1,8192,512]{2,1,0:T(8,128)(2,1)S(1)} %bitcast.180, f32[32,8192]{1,0:T(8,128)S(1)} %get-tuple-element.238, f32[32]{0:T(128)S(1)} %get-tuple-element.237), kind=kOutput, calls=%fused_computation.16 | convolution fusion | flops 268959744 | bytes 9502848 | tf_op jit(solution)/shard_map/shp,spk->shk/dot_general | solution.py:138
  41.4 7.1 %all-reduce.2 = (f32[128]{0:T(128)S(1)}, f32[128]{0:T(128)S(1)}) all-reduce(f32[128]{0:T(128)S(1)} %dynamic-update-slice, f32[128]{0:T(128)S(1)} %dynamic-update-slice.1), channel_id=3, replica_groups=mesh['sp'=8,'tp'=4] {'tp'}, use_global_device_ids=true, to_apply=%add | all-reduce | flops 256 | bytes 2048
  51.6 5.8 %all-gather.3 = f32[128,512]{1,0:T(8,128)S(1)} all-gather(f32[32,512]{1,0:T(8,128)S(1)} %fusion.9), channel_id=5, replica_groups=mesh['sp'=8,'tp'=4] {'tp'}, dimensions={0}, use_global_device_ids=true | all-gather | bytes 327680 | tf_op jit(solution)/shard_map/all_gather | solution.py:42
  57.4 7.6 %while.19 = (s32[]{:T(128)}, f32[1,32]{1,0:T(1,128)}, f32[1,32]{1,0:T(1,128)}, f32[1,32,512]{2,1,0:T(8,128)S(1)}, f32[4,1,32]{2,1,0:T(1,128)}, /*index=5*/f32[4,...) while((s32[]{:T(128)}, f32[1,32]{1,0:T(1,128)}, f32[1,32]{1,0:T(1,128)}, ...), condition=%wide.region_4.5_spmd, body=%wide.region_3.4_spmd.sunk | while | flops 49381 | bytes 198675 | solution.py:47
  66.9 1.4 %collective-permute-start.5 = (bf16[1,10,1024]{2,1,0:T(8,128)(2,1)S(1)}, bf16[1,10,1024]{2,1,0:T(8,128)(2,1)S(1)}, u32[]{:S(2)}, u32[]{:S(2)}) collective-permute-start(bf16[1,10,1024]{2,1,0:T(8,128)(2,1)S(1)} %copy.51), channel_id=1, source_target_pairs={{0,24},{4,28},{8,0},{12,4},{16,8},{20,12},{24,16},{28,20},{1,25},{... | collective-permute-start | bytes 61448 | tf_op jit(solution)/shard_map/ppermute | solution.py:34
  68.3 1.4 %bitcast_dynamic-update-slice_fusion.6 = bf16[8,1,10,1024]{3,2,1,0:T(8,128)(2,1)} fusion(bf16[8,1,10,1024]{3,2,1,0:T(8,128)(2,1)} %fusion.35, bf16[1,10,1024]{2,1,0:T(8,128)(2,1)} %collective-permute-done), kind=kLoop, calls=%fused_computation.57 | loop fusion | bytes 65536
  69.7 1.4 %collective-permute-start.6 = (bf16[1,10,1024]{2,1,0:T(8,128)(2,1)S(1)}, bf16[1,10,1024]{2,1,0:T(8,128)(2,1)S(1)}, u32[]{:S(2)}, u32[]{:S(2)}) collective-permute-start(bf16[1,10,1024]{2,1,0:T(8,128)(2,1)S(1)} %copy.52), channel_id=1, source_target_pairs={{0,28},{4,0},{8,4},{12,8},{16,12},{20,16},{24,20},{28,24},{1,29},{... | collective-permute-start | bytes 61448 | tf_op jit(solution)/shard_map/ppermute | solution.py:34
  71.1 1.4 %bitcast_dynamic-update-slice_fusion.5 = bf16[8,1,10,1024]{3,2,1,0:T(8,128)(2,1)} fusion(bf16[8,1,10,1024]{3,2,1,0:T(8,128)(2,1)} %bitcast_dynamic-update-slice_fusion.6, bf16[1,10,1024]{2,1,0:T(8,128)(2,1)} %collective-permute-done.1), kind=kLoop, calls=%fused_computation.56 | loop fusion | bytes 65536
  72.5 1.4 %bitcast_dynamic-update-slice_fusion.4 = bf16[8,1,10,1024]{3,2,1,0:T(8,128)(2,1)} fusion(bf16[8,1,10,1024]{3,2,1,0:T(8,128)(2,1)} %bitcast_dynamic-update-slice_fusion.5, bf16[1,10,1024]{2,1,0:T(8,128)(2,1)} %collective-permute-done.2), kind=kLoop, calls=%fused_computation.55 | loop fusion | bytes 65536
  73.9 1.4 %bitcast_dynamic-update-slice_fusion.3 = bf16[8,1,10,1024]{3,2,1,0:T(8,128)(2,1)} fusion(bf16[8,1,10,1024]{3,2,1,0:T(8,128)(2,1)} %bitcast_dynamic-update-slice_fusion.4, bf16[1,10,1024]{2,1,0:T(8,128)(2,1)} %collective-permute-done.3), kind=kLoop, calls=%fused_computation.54 | loop fusion | bytes 65536
  75.3 1.4 %bitcast_dynamic-update-slice_fusion.2 = bf16[8,1,10,1024]{3,2,1,0:T(8,128)(2,1)} fusion(bf16[8,1,10,1024]{3,2,1,0:T(8,128)(2,1)} %bitcast_dynamic-update-slice_fusion.3, bf16[1,10,1024]{2,1,0:T(8,128)(2,1)} %collective-permute-done.4), kind=kLoop, calls=%fused_computation.53 | loop fusion | bytes 65536
  77.9 1.6 %gather_fusion = bf16[8,10,1024]{2,1,0:T(8,128)(2,1)S(1)} fusion(bf16[8,10,1024]{2,1,0:T(8,128)(2,1)} %bitcast.182, s32[1024]{0:T(1024)} %pad_clamp_fusion), kind=kCustom, calls=%fused_computation | custom fusion | bytes 327712 | tf_op jit(solution)/shard_map/gather | solution.py:37
  80.2 7.6 %all_gather.27 = bf16[1,80,4096]{2,1,0:T(8,128)(2,1)S(1)} all-gather(bf16[1,80,1024]{2,1,0:T(8,128)(2,1)} %reshape_transpose.3), channel_id=1, replica_groups=mesh['sp'=8,'tp'=4] {'tp'}, dimensions={2}, use_global_device_ids=true | all-gather | bytes 819200 | tf_op jit(solution)/shard_map/all_gather | solution.py:94
  87.9 1.4 %convolution_bitcast_fusion = f32[1,80,64]{1,2,0:T(8,128)S(1)} fusion(bf16[4096,64]{0,1:T(8,128)(2,1)} %param.14, bf16[1,80,4096]{2,1,0:T(8,128)(2,1)S(1)} %all_gather.27), kind=kOutput, calls=%fused_computation.22 | convolution fusion | flops 41943040 | bytes 1200128 | tf_op jit(solution)/shard_map/dot_general | solution.py:98
  89.3 3.1 %multiply_reduce_fusion = (f32[80]{0:T(128)S(1)}, f32[80,512]{1,0:T(8,128)S(1)}) fusion(bf16[4096,512]{1,0:T(8,128)(2,1)} %param.13, bf16[1,80,4096]{2,1,0:T(8,128)(2,1)S(1)} %all_gather.27), kind=kOutput, calls=%fused_computation.47 | convolution fusion | flops 335626176 | bytes 5013824 | tf_op jit(solution)/shard_map/dot_general | solution.py:97
  (98 shorter events, 26.1 us)
Async XLA Ops:
  0.6 36.6 %copy-start = (bf16[1,8192,64]{1,2,0:T(8,128)(2,1)S(1)}, bf16[1,8192,64]{1,2,0:T(8,128)(2,1)}, u32[]{:S(2)}) copy-start(bf16[1,8192,64]{1,2,0:T(8,128)(2,1)} %param.19) | copy-start | bytes 3145732
  3.6 63.3 %collective-permute-start = (bf16[1,10,1024]{2,1,0:T(8,128)(2,1)}, bf16[1,10,1024]{2,1,0:T(8,128)(2,1)}, u32[]{:S(2)}, u32[]{:S(2)}) collective-permute-start(bf16[1,10,1024]{2,1,0:T(8,128)(2,1)} %copy.46), channel_id=1, source_target_pairs={{0,4},{4,8},{8,12},{12,16},{16,20},{20,24},{24,28},{28,0},{1,5},{5... | collective-permute-start | bytes 61448 | tf_op jit(solution)/shard_map/ppermute | solution.py:34
  7.2 62.5 %collective-permute-start.1 = (bf16[1,10,1024]{2,1,0:T(8,128)(2,1)}, bf16[1,10,1024]{2,1,0:T(8,128)(2,1)}, u32[]{:S(2)}, u32[]{:S(2)}) collective-permute-start(bf16[1,10,1024]{2,1,0:T(8,128)(2,1)} %copy.47), channel_id=1, source_target_pairs={{0,8},{4,12},{8,16},{12,20},{16,24},{20,28},{24,0},{28,4},{1,9},{5... | collective-permute-start | bytes 61448 | tf_op jit(solution)/shard_map/ppermute | solution.py:34
  9.4 63.1 %collective-permute-start.2 = (bf16[1,10,1024]{2,1,0:T(8,128)(2,1)}, bf16[1,10,1024]{2,1,0:T(8,128)(2,1)}, u32[]{:S(2)}, u32[]{:S(2)}) collective-permute-start(bf16[1,10,1024]{2,1,0:T(8,128)(2,1)} %copy.48), channel_id=1, source_target_pairs={{0,12},{4,16},{8,20},{12,24},{16,28},{20,0},{24,4},{28,8},{1,13},{... | collective-permute-start | bytes 61448 | tf_op jit(solution)/shard_map/ppermute | solution.py:34
  12.6 61.3 %collective-permute-start.3 = (bf16[1,10,1024]{2,1,0:T(8,128)(2,1)}, bf16[1,10,1024]{2,1,0:T(8,128)(2,1)}, u32[]{:S(2)}, u32[]{:S(2)}) collective-permute-start(bf16[1,10,1024]{2,1,0:T(8,128)(2,1)} %copy.49), channel_id=1, source_target_pairs={{0,16},{4,20},{8,24},{12,28},{16,0},{20,4},{24,8},{28,12},{1,17},{... | collective-permute-start | bytes 61448 | tf_op jit(solution)/shard_map/ppermute | solution.py:34
  14.4 60.8 %collective-permute-start.4 = (bf16[1,10,1024]{2,1,0:T(8,128)(2,1)}, bf16[1,10,1024]{2,1,0:T(8,128)(2,1)}, u32[]{:S(2)}, u32[]{:S(2)}) collective-permute-start(bf16[1,10,1024]{2,1,0:T(8,128)(2,1)} %copy.50), channel_id=1, source_target_pairs={{0,20},{4,24},{8,28},{12,0},{16,4},{20,8},{24,12},{28,16},{1,21},{... | collective-permute-start | bytes 61448 | tf_op jit(solution)/shard_map/ppermute | solution.py:34
  18.4 0.6 copy-start.7
  24.2 13.8 %slice-start = ((s8[8388608]{0:T(1024)(128)(4,1)}), s8[4194304]{0:T(1024)(128)(4,1)S(1)}, s32[]{:S(2)}) async-start(s8[8388608]{0:T(1024)(128)(4,1)} %bitcast.179), calls=%async_computation | async-start | bytes 8388608
  31.1 6.8 %slice-start.1 = ((s8[8388608]{0:T(1024)(128)(4,1)}), s8[4194304]{0:T(1024)(128)(4,1)S(1)}, s32[]{:S(2)}) async-start(s8[8388608]{0:T(1024)(128)(4,1)} %bitcast.179), calls=%async_computation.1 | async-start | bytes 8388608
  38.0 1.7 %copy-start.13 = (u32[32]{0:T(128)S(1)}, u32[32]{0:T(128)}, u32[]{:S(2)}) copy-start(u32[32]{0:T(128)} %constant.148) | copy-start | bytes 388
  39.6 52.8 %copy-start.1 = (bf16[512,1024]{1,0:T(8,128)(2,1)S(1)}, bf16[512,1024]{1,0:T(8,128)(2,1)}, u32[]{:S(2)}) copy-start(bf16[512,1024]{1,0:T(8,128)(2,1)} %param.16) | copy-start | bytes 3145732
  39.6 53.2 %copy-start.2 = (bf16[512,1024]{1,0:T(8,128)(2,1)S(1)}, bf16[512,1024]{1,0:T(8,128)(2,1)}, u32[]{:S(2)}) copy-start(bf16[512,1024]{1,0:T(8,128)(2,1)} %param.17) | copy-start | bytes 3145732
  66.8 25.6 %copy-start.8 = (f32[512]{0:T(512)S(1)}, f32[512]{0:T(512)}, u32[]{:S(2)}) copy-start(f32[512]{0:T(512)} %param.15) | copy-start | bytes 6148
  66.8 26.3 %copy-start.12 = (bf16[1,1024]{1,0:T(2,128)(2,1)S(1)}, bf16[1,1024]{1,0:T(2,128)(2,1)}, u32[]{:S(2)}) copy-start(bf16[1,1024]{1,0:T(2,128)(2,1)} %param.20) | copy-start | bytes 6148
  66.8 26.5 %copy-start.10 = (f32[80]{0:T(128)S(1)}, f32[80]{0:T(128)}, u32[]{:S(2)}) copy-start(f32[80]{0:T(128)} %add_convert_fusion) | copy-start | bytes 964
  66.9 26.5 %copy-start.11 = (f32[32]{0:T(128)S(1)}, f32[32]{0:T(128)}, u32[]{:S(2)}) copy-start(f32[32]{0:T(128)} %multiply_power_fusion) | copy-start | bytes 388
  66.9 27.3 %copy-start.9 = (bf16[8,64]{1,0:T(8,128)(2,1)S(1)}, bf16[8,64]{1,0:T(8,128)(2,1)}, u32[]{:S(2)}) copy-start(bf16[8,64]{1,0:T(8,128)(2,1)} %reshape.392) | copy-start | bytes 3076
  66.9 27.5 %copy-start.5 = (f32[1,32]{1,0:T(1,128)S(1)}, f32[1,32]{1,0:T(1,128)}, u32[]{:S(2)}) copy-start(f32[1,32]{1,0:T(1,128)} %get-tuple-element.183) | copy-start | bytes 388
  66.9 27.8 %copy-start.6 = (f32[1,32]{1,0:T(1,128)S(1)}, f32[1,32]{1,0:T(1,128)}, u32[]{:S(2)}) copy-start(f32[1,32]{1,0:T(1,128)} %get-tuple-element.184) | copy-start | bytes 388
  66.9 9.7 %collective-permute-start.5 = (bf16[1,10,1024]{2,1,0:T(8,128)(2,1)S(1)}, bf16[1,10,1024]{2,1,0:T(8,128)(2,1)S(1)}, u32[]{:S(2)}, u32[]{:S(2)}) collective-permute-start(bf16[1,10,1024]{2,1,0:T(8,128)(2,1)S(1)} %copy.51), channel_id=1, source_target_pairs={{0,24},{4,28},{8,0},{12,4},{16,8},{20,12},{24,16},{28,20},{1,25},{... | collective-permute-start | bytes 61448 | tf_op jit(solution)/shard_map/ppermute | solution.py:34
  69.7 7.6 %collective-permute-start.6 = (bf16[1,10,1024]{2,1,0:T(8,128)(2,1)S(1)}, bf16[1,10,1024]{2,1,0:T(8,128)(2,1)S(1)}, u32[]{:S(2)}, u32[]{:S(2)}) collective-permute-start(bf16[1,10,1024]{2,1,0:T(8,128)(2,1)S(1)} %copy.52), channel_id=1, source_target_pairs={{0,28},{4,0},{8,4},{12,8},{16,12},{20,16},{24,20},{28,24},{1,29},{... | collective-permute-start | bytes 61448 | tf_op jit(solution)/shard_map/ppermute | solution.py:34
  92.8 3.2 %copy-start.3 = (bf16[80,1024]{1,0:T(8,128)(2,1)}, bf16[80,1024]{1,0:T(8,128)(2,1)S(1)}, u32[]{:S(2)}) copy-start(bf16[80,1024]{1,0:T(8,128)(2,1)S(1)} %convolution_convert_fusion.1) | copy-start | bytes 491524
  93.2 2.8 %copy-start.4 = (bf16[80,1024]{1,0:T(8,128)(2,1)}, bf16[80,1024]{1,0:T(8,128)(2,1)S(1)}, u32[]{:S(2)}) copy-start(bf16[80,1024]{1,0:T(8,128)(2,1)S(1)} %convolution_convert_fusion) | copy-start | bytes 491524
